TPU v7x, 32 devices: a whole 2x2x4 slice. The times are simulated.
32 devices in a mesh: fs: 16 (over z, y, core), tp: 2 (over x).
Axes of the slice: x: 2, y: 2, z: 4, core: 2. Of those that a mesh axis runs over, the one named last changes fastest.
Arguments:
- inputs: bfloat16 [16384, 3072], P('fs'), may hold values from -6 to 6
- query_cot: bfloat16 [16384, 768], P('fs', 'tp'), may hold values from -0.046875 to 0.046875
- value_cot: bfloat16 [16384, 1536], P('fs', 'tp'), may hold values from -0.046875 to 0.046875
- query_factor: bfloat16 [3072, 192], P('fs'), may hold values from -0.109375 to 0.109375
- value_factor: bfloat16 [3072, 192], P('fs'), may hold values from -0.109375 to 0.109375
- query_weight: float32 [3072, 768], P('fs', 'tp'), may hold values from -0.109375 to 0.109375
- value_weight: float32 [3072, 1536], P('fs', 'tp'), may hold values from -0.109375 to 0.109375
- query_first: float32 [192, 768], P('fs', 'tp'), may hold values from -1.6 to 1.6
- query_second: float32 [192, 768], P('fs', 'tp'), may hold values from 0.002 to 0.05
- value_first: float32 [192, 1536], P('fs', 'tp'), may hold values from -1.6 to 1.6
- value_second: float32 [192, 1536], P('fs', 'tp'), may hold values from 0.002 to 0.05
Outputs:
- step_q: float32 [3072, 768], P('fs', 'tp')
- step_v: float32 [3072, 1536], P('fs', 'tp')
- new_q: float32 [3072, 768], P('fs', 'tp')
- new_v: float32 [3072, 1536], P('fs', 'tp')
- first_q: float32 [192, 768], P('fs', 'tp')
- second_q: float32 [192, 768], P('fs', 'tp')
- first_v: float32 [192, 1536], P('fs', 'tp')
- second_v: float32 [192, 1536], P('fs', 'tp')
- copy_q: bfloat16 [3072, 768], P(None, 'tp')
- copy_v: bfloat16 [3072, 1536], P(None, 'tp')
All inputs are finite; a program needn't handle non-finite values.
Results may differ from a plain program's by a relative error of at most 0.0041.
Values may be sent and summed in bfloat16 or wider, within the bound.
A program may use at most 64 MiB of HBM per device.

v0:
```python
import jax
import jax.numpy as jnp
from jax import lax
from jax.sharding import PartitionSpec as P

first_decay = 0.9
second_decay = 0.99
small_eps = 1e-08
learn_rate = 0.01


def moments(old_first, old_second, gradient):
    first = first_decay * old_first + (1.0 - first_decay) * gradient
    second = second_decay * old_second + (1.0 - second_decay) * gradient * gradient
    unit = first / (jnp.sqrt(second) + small_eps)
    return (first, second, unit)


def on_device(
    inputs,
    query_cot,
    value_cot,
    query_factor,
    value_factor,
    query_weight,
    value_weight,
    query_first,
    query_second,
    value_first,
    value_second,
):
    rank_cols = query_factor.shape[1]
    q_cols = query_cot.shape[1]
    v_cols = value_cot.shape[1]
    own_rows = query_first.shape[0]
    entries = rank_cols * (q_cols + v_cols) * lax.axis_size("tp")
    full_qf, full_vf = (
        lax.all_gather(query_factor, "fs", axis=0, tiled=True),
        lax.all_gather(value_factor, "fs", axis=0, tiled=True),
    )
    sum_q = jnp.dot(inputs, full_qf, preferred_element_type=jnp.float32)
    sum_v = jnp.dot(inputs, full_vf, preferred_element_type=jnp.float32)
    proj_q = sum_q.astype(jnp.bfloat16)
    proj_v = sum_v.astype(jnp.bfloat16)
    term_q = lax.dot_general(
        proj_q, query_cot, (((0,), (0,)), ((), ())), preferred_element_type=jnp.float32
    )
    term_v = lax.dot_general(
        proj_v, value_cot, (((0,), (0,)), ((), ())), preferred_element_type=jnp.float32
    )
    full_sums = lax.psum(jnp.concatenate([term_q, term_v], axis=1), "fs")
    stacked = (
        lax.all_gather(query_first, "fs", axis=0, tiled=True),
        lax.all_gather(query_second, "fs", axis=0, tiled=True),
        lax.all_gather(value_first, "fs", axis=0, tiled=True),
        lax.all_gather(value_second, "fs", axis=0, tiled=True),
    )
    all_first_q, all_second_q, unit_q = moments(stacked[0], stacked[1], full_sums[:, :q_cols])
    all_first_v, all_second_v, unit_v = moments(stacked[2], stacked[3], full_sums[:, q_cols:])
    norm_total = lax.psum(jnp.sum(unit_q * unit_q) + jnp.sum(unit_v * unit_v), "tp")
    step_scale = lax.rsqrt(norm_total / entries + 1e-06)
    whole_q = (step_scale * unit_q).astype(jnp.bfloat16)
    whole_v = (step_scale * unit_v).astype(jnp.bfloat16)
    row_begin = lax.axis_index("fs") * own_rows
    first_q = lax.dynamic_slice_in_dim(all_first_q, row_begin, own_rows, 0)
    second_q = lax.dynamic_slice_in_dim(all_second_q, row_begin, own_rows, 0)
    first_v = lax.dynamic_slice_in_dim(all_first_v, row_begin, own_rows, 0)
    second_v = lax.dynamic_slice_in_dim(all_second_v, row_begin, own_rows, 0)
    step_q = jnp.dot(query_factor, whole_q, preferred_element_type=jnp.float32)
    step_v = jnp.dot(value_factor, whole_v, preferred_element_type=jnp.float32)
    new_q = query_weight - learn_rate * step_q
    new_v = value_weight - learn_rate * step_v
    copy_q, copy_v = (
        lax.all_gather(new_q.astype(jnp.bfloat16), "fs", axis=0, tiled=True),
        lax.all_gather(new_v.astype(jnp.bfloat16), "fs", axis=0, tiled=True),
    )
    return (step_q, step_v, new_q, new_v, first_q, second_q, first_v, second_v, copy_q, copy_v)


def solution(mesh):
    in_specs = (
        P("fs", None),
        P("fs", "tp"),
        P("fs", "tp"),
        P("fs", None),
        P("fs", None),
        P("fs", "tp"),
        P("fs", "tp"),
        P("fs", "tp"),
        P("fs", "tp"),
        P("fs", "tp"),
        P("fs", "tp"),
    )
    out_specs = (
        P("fs", "tp"),
        P("fs", "tp"),
        P("fs", "tp"),
        P("fs", "tp"),
        P("fs", "tp"),
        P("fs", "tp"),
        P("fs", "tp"),
        P("fs", "tp"),
        P(None, "tp"),
        P(None, "tp"),
    )
    return jax.shard_map(
        on_device, mesh=mesh, in_specs=in_specs, out_specs=out_specs, check_vma=False
    )
```

profile of v0, /device:TPU:0, one launch (start us, length us, event | category | flops | bytes accessed | tf_op | source)
XLA Modules:
  0.0 321.6 jit_solution(11538157095303594677)
XLA Ops:
  7.2 0.0 copy-start
  7.2 0.0 copy-start.8
  7.2 0.0 all-gather.11.cloned.1.call-start
  7.2 0.7 all-gather.11.cloned.1.call-update
  7.9 0.0 all-gather.9.cloned.1.call-start
  8.0 0.7 all-gather.9.cloned.1.call-update
  8.7 0.0 all-reduce.2.cloned.1.call-start
  8.7 24.6 %all-gather = f32[16,12,384]{2,1,0:T(8,128)S(1)} all-gather(f32[1,12,384]{2,1,0:T(8,128)} %bitcast.18), channel_id=1, replica_groups=mesh['fs'=16,'tp'=2] {'fs'}, dimensions={0}, use_global_device_ids=true | all-gather | bytes 313344 | tf_op jit(solution)/shard_map/all_gather | solution.py:53
  33.4 21.9 %all-gather.2 = f32[16,12,768]{2,1,0:T(8,128)S(1)} all-gather(f32[1,12,768]{2,1,0:T(8,128)} %bitcast.16), channel_id=1, replica_groups=mesh['fs'=16,'tp'=2] {'fs'}, dimensions={0}, use_global_device_ids=true | all-gather | bytes 626688 | tf_op jit(solution)/shard_map/all_gather | solution.py:55
  55.3 0.1 broadcast_multiply_fusion.1
  55.4 0.0 copy-done.8
  55.4 21.1 %all-gather.3 = f32[16,12,768]{2,1,0:T(8,128)S(1)} all-gather(f32[1,12,768]{2,1,0:T(8,128)S(1)} %bitcast.17), channel_id=1, replica_groups=mesh['fs'=16,'tp'=2] {'fs'}, dimensions={0}, use_global_device_ids=true | all-gather | bytes 626688 | tf_op jit(solution)/shard_map/all_gather | solution.py:56
  76.5 0.1 broadcast_multiply_fusion
  76.6 0.0 all-gather.11.cloned.1.call-done
  76.6 0.0 copy-done
  76.6 6.6 %fusion.1 = f32[192,768]{1,0:T(8,128)} fusion(bf16[1024,768]{1,0:T(8,128)(2,1)S(1)} %copy-done, bf16[1024,3072]{1,0:T(8,128)(2,1)} %param.11, bf16[3072,192]{1,0:T(8,128)(2,1)} %all-gather.11.cloned.1.call-done), kind=kOutput, calls=%fused_computation.5 | convolution fusion | flops 1510146048 | bytes 9633792 | tf_op jit(solution)/shard_map/dot_general | solution.py:48
  83.3 15.3 %all-gather.9.cloned.1.call-done = bf16[3072,192]{1,0:T(8,128)(2,1)} async-done(((bf16[192,192]{1,0:T(8,128)(2,1)}), bf16[3072,192]{1,0:T(8,128)(2,1)}) %all-gather.9.cloned.1.call-update) | async-done | bytes 1179664 | tf_op jit(solution)/shard_map/all_gather | solution.py:38
  98.5 6.5 %fusion = f32[192,384]{1,0:T(8,128)} fusion(bf16[1024,384]{1,0:T(8,128)(2,1)} %param.12, bf16[1024,3072]{1,0:T(8,128)(2,1)} %param.11, bf16[3072,192]{1,0:T(8,128)(2,1)} %all-gather.9.cloned.1.call-done), kind=kOutput, calls=%fused_computation.4 | convolution fusion | flops 1359151104 | bytes 8552448 | tf_op jit(solution)/shard_map/dot_general | solution.py:45
  105.0 2.1 pad_maximum_fusion
  107.2 0.0 all-reduce.2.cloned.1.call-update
  107.2 0.0 all-gather.13.cloned.1.call-start
  107.2 0.8 broadcast_multiply_fusion.3
  108.0 0.9 reshape.33
  108.9 0.0 copy-start.3
  108.9 0.0 copy-start.9
  108.9 0.9 reshape.35
  109.8 0.2 copy-done.3
  110.0 0.0 copy-start.2
  110.0 0.7 reshape.29
  110.7 0.0 copy-done.9
  110.7 20.7 %all-gather.1 = f32[16,12,384]{2,1,0:T(8,128)S(1)} all-gather(f32[1,12,384]{2,1,0:T(8,128)S(1)} %bitcast.19), channel_id=1, replica_groups=mesh['fs'=16,'tp'=2] {'fs'}, dimensions={0}, use_global_device_ids=true | all-gather | bytes 313344 | tf_op jit(solution)/shard_map/all_gather | solution.py:54
  131.4 0.7 reshape.31
  132.2 0.0 copy-start.7
  132.2 67.6 %all-reduce.2.cloned.1.call-done = f32[192,1152]{1,0:T(8,128)} async-done(((f32[192,1152]{1,0:T(8,128)}), f32[192,1152]{1,0:T(8,128)}) %all-reduce.2.cloned.1.call-update) | async-done | bytes 884752 | tf_op jit(solution)/shard_map/psum | solution.py:51
  199.7 0.0 copy-done.2
  199.7 0.0 copy-start.4
  199.7 0.0 copy-start.5
  199.7 2.2 multiply_reduce_fusion
  202.0 0.0 copy-done.4
  202.0 0.0 copy-done.5
  202.0 0.0 copy-start.6
  202.0 1.8 multiply_reduce_fusion.1
  205.1 5.4 %psum.15 = f32[]{:T(128)} all-reduce(f32[]{:T(128)S(6)} %add.48), channel_id=1, replica_groups=mesh['fs'=16,'tp'=2] {'tp'}, use_global_device_ids=true, to_apply=%region_3.0 | all-reduce | flops 1 | bytes 8 | tf_op jit(solution)/shard_map/psum | solution.py:60
  211.2 0.0 copy-done.7
  211.2 2.1 fusion.7
  213.3 0.0 all-gather.13.cloned.1.call-update
  213.3 0.0 all-gather.15.cloned.1.call-start
  213.4 0.0 copy-done.6
  213.4 2.6 fusion.6
  216.0 0.0 all-gather.15.cloned.1.call-update
  216.0 0.6 constant_dynamic-slice_fusion.2
  216.7 0.6 constant_dynamic-slice_fusion
  217.3 37.5 %all-gather.13.cloned.1.call-done = bf16[3072,384]{1,0:T(8,128)(2,1)} async-done(((bf16[192,384]{1,0:T(8,128)(2,1)}), bf16[3072,384]{1,0:T(8,128)(2,1)}) %all-gather.13.cloned.1.call-update) | async-done | bytes 2359312 | tf_op jit(solution)/shard_map/all_gather | solution.py:74
  254.8 54.6 %all-gather.15.cloned.1.call-done = bf16[3072,768]{1,0:T(8,128)(2,1)} async-done(((bf16[192,768]{1,0:T(8,128)(2,1)}), bf16[3072,768]{1,0:T(8,128)(2,1)}) %all-gather.15.cloned.1.call-update) | async-done | bytes 4718608 | tf_op jit(solution)/shard_map/all_gather | solution.py:75
  309.4 0.0 copy-start.1
  309.4 3.5 %copy.24 = bf16[3072,384]{1,0:T(8,128)(2,1)} copy(bf16[3072,384]{1,0:T(8,128)(2,1)} %all-gather.13.cloned.1.call-done) | data formatting | bytes 4718592
  312.8 0.0 copy-done.1
  312.8 2.2 copy.25
  (1 shorter events, 0.0 us)
Async XLA Ops:
  7.2 69.5 %copy-start = (bf16[1024,768]{1,0:T(8,128)(2,1)S(1)}, bf16[1024,768]{1,0:T(8,128)(2,1)}, u32[]{:S(2)}) copy-start(bf16[1024,768]{1,0:T(8,128)(2,1)} %param.13) | copy-start | bytes 4718596
  7.2 48.2 %copy-start.8 = (f32[12,768]{1,0:T(8,128)S(1)}, f32[12,768]{1,0:T(8,128)}, u32[]{:S(2)}) copy-start(f32[12,768]{1,0:T(8,128)} %param.21) | copy-start | bytes 110596
  7.2 69.4 %all-gather.11.cloned.1.call-start = ((), (), s32[]{:S(2)}) async-start(), calls=%async_computation.1 | async-start | bytes 1671168 | tf_op jit(solution)/shard_map/all_gather | solution.py:39
  7.9 90.6 %all-gather.9.cloned.1.call-start = ((), (), s32[]{:S(2)}) async-start(), calls=%async_computation | async-start | bytes 1671168 | tf_op jit(solution)/shard_map/all_gather | solution.py:38
  8.7 191.0 %all-reduce.2.cloned.1.call-start = ((), (), s32[]{:S(2)}) async-start(), calls=%async_computation.2 | async-start | bytes 1769472 | tf_op jit(solution)/shard_map/psum | solution.py:51
  107.2 147.6 %all-gather.13.cloned.1.call-start = ((), (), s32[]{:S(2)}) async-start(), calls=%async_computation.3 | async-start | bytes 2506752 | tf_op jit(solution)/shard_map/all_gather | solution.py:74
  108.9 1.1 copy-start.3
  108.9 1.8 copy-start.9
  110.0 89.8 %copy-start.2 = (f32[192,768]{1,0:T(8,128)S(1)}, f32[192,768]{1,0:T(8,128)}, u32[]{:S(2)}) copy-start(f32[192,768]{1,0:T(8,128)} %reshape.33) | copy-start | bytes 1769476
  132.2 79.0 %copy-start.7 = (bf16[192,192]{1,0:T(8,128)(2,1)S(1)}, bf16[192,192]{1,0:T(8,128)(2,1)}, u32[]{:S(2)}) copy-start(bf16[192,192]{1,0:T(8,128)(2,1)} %param.14) | copy-start | bytes 221188
  199.7 2.2 copy-start.4
  199.7 2.2 copy-start.5
  202.0 11.4 %copy-start.6 = (bf16[192,192]{1,0:T(8,128)(2,1)S(1)}, bf16[192,192]{1,0:T(8,128)(2,1)}, u32[]{:S(2)}) copy-start(bf16[192,192]{1,0:T(8,128)(2,1)} %param.15) | copy-start | bytes 221188
  213.3 96.0 %all-gather.15.cloned.1.call-start = ((), (), s32[]{:S(2)}) async-start(), calls=%async_computation.4 | async-start | bytes 5013504 | tf_op jit(solution)/shard_map/all_gather | solution.py:75
  309.4 3.5 %copy-start.1 = (bf16[3072,768]{1,0:T(8,128)(2,1)S(1)}, bf16[3072,768]{1,0:T(8,128)(2,1)}, u32[]{:S(2)}) copy-start(bf16[3072,768]{1,0:T(8,128)(2,1)} %all-gather.15.cloned.1.call-done) | copy-start | bytes 14155780
Sparse Core Ops, SparseCore 0:
  10.3 43.8 all-gather.10
  56.4 42.0 all-gather.8
  107.3 92.3 all-reduce.1
  213.5 41.3 all-gather.12
  257.5 51.8 all-gather.14
where the time goes:
time: 322 us
  waiting for transfers between devices  176 us (55%)
  blocking collectives  93.8 us (29%)
  matrix products  17.9 us (6%)
  between operations  15.9 us (5%)
  local copies, waits for them, and re-layouts  10.4 us (3%)
  other arithmetic  7.08 us (2%)
    psum x1, waiting for transfers between devices, on_device(): full_sums = lax.psum(jnp.concatenate([term_q, term_v], axis=1), 'fs')  67.6 us
    all_gather x1, waiting for transfers between devices, on_device(): lax.all_gather(new_v.astype(jnp.bfloat16), 'fs', axis=0, tiled=True)  54.6 us
    all_gather x1, waiting for transfers between devices, on_device(): lax.all_gather(new_q.astype(jnp.bfloat16), 'fs', axis=0, tiled=True)  37.5 us
    all_gather x1, blocking collectives, on_device(): lax.all_gather(query_first, 'fs', axis=0, tiled=True)  24.6 us
    all_gather x1, blocking collectives, on_device(): lax.all_gather(value_first, 'fs', axis=0, tiled=True)  21.9 us
    all_gather x1, blocking collectives, on_device(): lax.all_gather(value_second, 'fs', axis=0, tiled=True)  21.1 us
    all_gather x1, blocking collectives, on_device(): lax.all_gather(query_second, 'fs', axis=0, tiled=True)  20.7 us
    all_gather x1, waiting for transfers between devices, on_device(): lax.all_gather(query_factor, 'fs', axis=0, tiled=True)  15.3 us
  transfers between devices with their start and end apart: 5, of which 4 were waited for; matrix products, arithmetic and copies ran while one was open for 5% of the time, Pallas kernels for 0%

commit v1 on v0

--- a/solution.py
+++ b/solution.py
@@ -1,3 +1,4 @@
+import functools
 import jax
 import jax.numpy as jnp
 from jax import lax
@@ -7,6 +8,15 @@
 second_decay = 0.99
 small_eps = 1e-08
 learn_rate = 0.01
+
+
+def _start_hubs(page, chip_axis):
+    formed = jnp.stack([page for _ in range(lax.axis_size(chip_axis))])
+    everything = lax.all_to_all(formed, chip_axis, 0, 0)
+    return jnp.concatenate(everything, axis=0)
+
+
+extend_zone_all = functools.partial(_start_hubs, chip_axis="fs")
 
 
 def moments(old_first, old_second, gradient):
@@ -72,7 +82,7 @@
     new_v = value_weight - learn_rate * step_v
     copy_q, copy_v = (
         lax.all_gather(new_q.astype(jnp.bfloat16), "fs", axis=0, tiled=True),
-        lax.all_gather(new_v.astype(jnp.bfloat16), "fs", axis=0, tiled=True),
+        extend_zone_all(new_v.astype(jnp.bfloat16)),
     )
     return (step_q, step_v, new_q, new_v, first_q, second_q, first_v, second_v, copy_q, copy_v)
 

time: 322 us -> 353 us (1.096)
  the two profiles are of different devices: /device:TPU:0 before, /device:TPU:13 now
where the time goes in v1:
time: 353 us
  waiting for transfers between devices  201 us (57%)
  blocking collectives  86.6 us (25%)
  matrix products  17.8 us (5%)
  between operations  15.9 us (5%)
  local copies, waits for them, and re-layouts  15.3 us (4%)
  starting transfers between devices  8.9 us (3%)
  other arithmetic  7.12 us (2%)
    all_gather x1, waiting for transfers between devices, on_device(): lax.all_gather(new_q.astype(jnp.bfloat16), 'fs', axis=0, tiled=True)  91.2 us
    psum x1, waiting for transfers between devices, on_device(): full_sums = lax.psum(jnp.concatenate([term_q, term_v], axis=1), 'fs')  69.2 us
    all_gather x1, blocking collectives, on_device(): lax.all_gather(value_first, 'fs', axis=0, tiled=True)  26.4 us
    all_to_all x1, waiting for transfers between devices, _start_hubs(): everything = lax.all_to_all(formed, chip_axis, 0, 0)  23.2 us
    all_gather x1, blocking collectives, on_device(): lax.all_gather(value_second, 'fs', axis=0, tiled=True)  20.6 us
    all_gather x1, blocking collectives, on_device(): lax.all_gather(query_second, 'fs', axis=0, tiled=True)  18.4 us
    all_gather x1, blocking collectives, on_device(): lax.all_gather(query_first, 'fs', axis=0, tiled=True)  16.9 us
    all_gather x1, waiting for transfers between devices, on_device(): lax.all_gather(query_factor, 'fs', axis=0, tiled=True)  15.9 us
  transfers between devices with their start and end apart: 5, of which 4 were waited for; matrix products, arithmetic and copies ran while one was open for 4% of the time, Pallas kernels for 0%

profile of v1, /device:TPU:13, one launch (start us, length us, event | category | flops | bytes accessed | tf_op | source)
XLA Modules:
  0.0 352.6 jit_solution(1083909091659549428)
XLA Ops:
  7.2 0.0 copy-start
  7.2 0.0 copy-start.6
  7.2 0.0 all-gather.10.cloned.1.call-start
  7.2 0.7 all-gather.10.cloned.1.call-update
  7.9 0.0 all-gather.8.cloned.1.call-start
  8.0 0.7 all-gather.8.cloned.1.call-update
  8.7 0.0 all-reduce.2.cloned.1.call-start
  8.7 16.9 %all-gather = f32[16,12,384]{2,1,0:T(8,128)S(1)} all-gather(f32[1,12,384]{2,1,0:T(8,128)} %bitcast.19), channel_id=1, replica_groups=mesh['fs'=16,'tp'=2] {'fs'}, dimensions={0}, use_global_device_ids=true | all-gather | bytes 313344 | tf_op jit(solution)/shard_map/all_gather | solution.py:63
  25.7 26.4 %all-gather.2 = f32[16,12,768]{2,1,0:T(8,128)S(1)} all-gather(f32[1,12,768]{2,1,0:T(8,128)} %bitcast.17), channel_id=1, replica_groups=mesh['fs'=16,'tp'=2] {'fs'}, dimensions={0}, use_global_device_ids=true | all-gather | bytes 626688 | tf_op jit(solution)/shard_map/all_gather | solution.py:65
  52.1 0.1 broadcast_multiply_fusion.1
  52.2 0.0 copy-done.6
  52.2 20.6 %all-gather.3 = f32[16,12,768]{2,1,0:T(8,128)S(1)} all-gather(f32[1,12,768]{2,1,0:T(8,128)S(1)} %bitcast.18), channel_id=1, replica_groups=mesh['fs'=16,'tp'=2] {'fs'}, dimensions={0}, use_global_device_ids=true | all-gather | bytes 626688 | tf_op jit(solution)/shard_map/all_gather | solution.py:66
  72.8 0.1 broadcast_multiply_fusion
  72.8 0.0 all-gather.10.cloned.1.call-done
  72.9 0.0 copy-done
  72.9 6.6 %fusion.1 = f32[192,768]{1,0:T(8,128)} fusion(bf16[1024,768]{1,0:T(8,128)(2,1)S(1)} %copy-done, bf16[1024,3072]{1,0:T(8,128)(2,1)} %param.11, bf16[3072,192]{1,0:T(8,128)(2,1)} %all-gather.10.cloned.1.call-done), kind=kOutput, calls=%fused_computation.5 | convolution fusion | flops 1510146048 | bytes 9633792 | tf_op jit(solution)/shard_map/dot_general | solution.py:58
  79.5 15.9 %all-gather.8.cloned.1.call-done = bf16[3072,192]{1,0:T(8,128)(2,1)} async-done(((bf16[192,192]{1,0:T(8,128)(2,1)}), bf16[3072,192]{1,0:T(8,128)(2,1)}) %all-gather.8.cloned.1.call-update) | async-done | bytes 1179664 | tf_op jit(solution)/shard_map/all_gather | solution.py:48
  95.4 6.5 %fusion = f32[192,384]{1,0:T(8,128)} fusion(bf16[1024,384]{1,0:T(8,128)(2,1)} %param.12, bf16[1024,3072]{1,0:T(8,128)(2,1)} %param.11, bf16[3072,192]{1,0:T(8,128)(2,1)} %all-gather.8.cloned.1.call-done), kind=kOutput, calls=%fused_computation.4 | convolution fusion | flops 1359151104 | bytes 8552448 | tf_op jit(solution)/shard_map/dot_general | solution.py:55
  102.0 2.1 pad_maximum_fusion
  104.1 0.0 all-reduce.2.cloned.1.call-update
  104.1 0.8 broadcast_multiply_fusion.3
  104.9 0.0 copy-start.2
  104.9 0.9 reshape.39
  105.8 0.9 reshape.41
  106.6 0.0 copy-done.2
  106.6 0.0 copy-start.1
  106.6 0.7 reshape.35
  107.4 18.4 %all-gather.1 = f32[16,12,384]{2,1,0:T(8,128)S(1)} all-gather(f32[1,12,384]{2,1,0:T(8,128)} %bitcast.20), channel_id=1, replica_groups=mesh['fs'=16,'tp'=2] {'fs'}, dimensions={0}, use_global_device_ids=true | all-gather | bytes 313344 | tf_op jit(solution)/shard_map/all_gather | solution.py:64
  125.9 0.7 reshape.37
  126.6 0.0 copy-start.4
  126.6 69.2 %all-reduce.2.cloned.1.call-done = f32[192,1152]{1,0:T(8,128)} async-done(((f32[192,1152]{1,0:T(8,128)}), f32[192,1152]{1,0:T(8,128)}) %all-reduce.2.cloned.1.call-update) | async-done | bytes 884752 | tf_op jit(solution)/shard_map/psum | solution.py:61
  195.8 0.0 copy-done.1
  195.8 0.0 copy-start.3
  195.8 2.2 multiply_reduce_fusion
  198.0 0.0 copy-done.3
  198.0 1.8 multiply_reduce_fusion.1
  201.2 4.3 %psum.15 = f32[]{:T(128)} all-reduce(f32[]{:T(128)S(6)} %add.48), channel_id=1, replica_groups=mesh['fs'=16,'tp'=2] {'tp'}, use_global_device_ids=true, to_apply=%region_3.0 | all-reduce | flops 1 | bytes 8 | tf_op jit(solution)/shard_map/psum | solution.py:70
  206.1 0.0 copy-done.4
  206.1 2.5 fusion.6
  208.7 2.6 stack.2
  211.3 0.0 copy-start.5
  211.3 8.7 %all-to-all-start = ((bf16[16,192,768]{2,1,0:T(8,128)(2,1)}), bf16[16,192,768]{2,1,0:T(8,128)(2,1)}, u32[]{:S(2)}, u32[]{:S(2)}) async-start(bf16[16,192,768]{2,1,0:T(8,128)(2,1)} %stack.2), calls=%async_computation | async-start | bytes 9437184 | tf_op jit(solution)/shard_map/all_to_all | solution.py:15
  220.0 0.0 all-gather.12.cloned.1.call-start
  220.1 0.0 copy-done.5
  220.1 2.1 fusion.7
  222.2 0.0 all-gather.12.cloned.1.call-update
  222.3 0.6 constant_dynamic-slice_fusion.2
  222.9 0.6 constant_dynamic-slice_fusion
  223.5 91.2 %all-gather.12.cloned.1.call-done = bf16[3072,384]{1,0:T(8,128)(2,1)} async-done(((bf16[192,384]{1,0:T(8,128)(2,1)}), bf16[3072,384]{1,0:T(8,128)(2,1)}) %all-gather.12.cloned.1.call-update) | async-done | bytes 2359312 | tf_op jit(solution)/shard_map/all_gather | solution.py:84
  314.7 23.2 %all-to-all-done = bf16[16,192,768]{2,1,0:T(8,128)(2,1)} async-done(((bf16[16,192,768]{2,1,0:T(8,128)(2,1)}), bf16[16,192,768]{2,1,0:T(8,128)(2,1)}, u32[]{:S(2)}, u32[]{:S(2)}) %all-to-all-start) | async-done | bytes 4718624 | tf_op jit(solution)/shard_map/all_to_all | solution.py:15
  337.9 3.3 copy.24
  341.2 4.8 %copy.25 = bf16[3072,768]{1,0:T(8,128)(2,1)} copy(bf16[3072,768]{1,0:T(8,128)(2,1)} %bitcast.6) | data formatting | bytes 9437184
  (1 shorter events, 0.0 us)
Async XLA Ops:
  7.2 65.7 %copy-start = (bf16[1024,768]{1,0:T(8,128)(2,1)S(1)}, bf16[1024,768]{1,0:T(8,128)(2,1)}, u32[]{:S(2)}) copy-start(bf16[1024,768]{1,0:T(8,128)(2,1)} %param.13) | copy-start | bytes 4718596
  7.2 45.0 %copy-start.6 = (f32[12,768]{1,0:T(8,128)S(1)}, f32[12,768]{1,0:T(8,128)}, u32[]{:S(2)}) copy-start(f32[12,768]{1,0:T(8,128)} %param.21) | copy-start | bytes 110596
  7.2 65.7 %all-gather.10.cloned.1.call-start = ((), (), s32[]{:S(2)}) async-start(), calls=%async_computation.2 | async-start | bytes 1671168 | tf_op jit(solution)/shard_map/all_gather | solution.py:49
  7.9 87.5 %all-gather.8.cloned.1.call-start = ((), (), s32[]{:S(2)}) async-start(), calls=%async_computation.1 | async-start | bytes 1671168 | tf_op jit(solution)/shard_map/all_gather | solution.py:48
  8.7 187.1 %all-reduce.2.cloned.1.call-start = ((), (), s32[]{:S(2)}) async-start(), calls=%async_computation.3 | async-start | bytes 1769472 | tf_op jit(solution)/shard_map/psum | solution.py:61
  104.9 1.8 copy-start.2
  106.6 89.2 %copy-start.1 = (f32[192,768]{1,0:T(8,128)S(1)}, f32[192,768]{1,0:T(8,128)}, u32[]{:S(2)}) copy-start(f32[192,768]{1,0:T(8,128)} %reshape.39) | copy-start | bytes 1769476
  126.6 79.5 %copy-start.4 = (bf16[192,192]{1,0:T(8,128)(2,1)S(1)}, bf16[192,192]{1,0:T(8,128)(2,1)}, u32[]{:S(2)}) copy-start(bf16[192,192]{1,0:T(8,128)(2,1)} %param.15) | copy-start | bytes 221188
  195.8 2.2 copy-start.3
  211.3 8.8 %copy-start.5 = (bf16[192,192]{1,0:T(8,128)(2,1)S(1)}, bf16[192,192]{1,0:T(8,128)(2,1)}, u32[]{:S(2)}) copy-start(bf16[192,192]{1,0:T(8,128)(2,1)} %param.14) | copy-start | bytes 221188
  211.3 126.6 %all-to-all-start = ((bf16[16,192,768]{2,1,0:T(8,128)(2,1)}), bf16[16,192,768]{2,1,0:T(8,128)(2,1)}, u32[]{:S(2)}, u32[]{:S(2)}) async-start(bf16[16,192,768]{2,1,0:T(8,128)(2,1)} %stack.2), calls=%async_computation | async-start | bytes 9437184 | tf_op jit(solution)/shard_map/all_to_all | solution.py:15
  220.0 94.7 %all-gather.12.cloned.1.call-start = ((), (), s32[]{:S(2)}) async-start(), calls=%async_computation.4 | async-start | bytes 2506752 | tf_op jit(solution)/shard_map/all_gather | solution.py:84
Sparse Core Ops, SparseCore 0:
  10.3 43.6 all-gather.9
  56.2 39.1 all-gather.7
  104.2 91.5 all-reduce.1
  223.4 91.2 all-gather.11
